TPU v7x, 32 devices: a whole 2x2x4 slice. The times are simulated.
32 devices in a mesh: grp: 2 (over x), sp: 8 (over z, y), tp: 2 (over core).
Axes of the slice: x: 2, y: 2, z: 4, core: 2. Of those that a mesh axis runs over, the one named last changes fastest.
Arguments:
- tokens: bfloat16 [8192, 2048], P(('grp', 'sp', 'tp')), parts along dimension 0, may hold values from -60 to 60
- query_weight: bfloat16 [2048, 1024], P(None, 'tp'), may hold values from -0.125 to 0.125
- key_weight: bfloat16 [2048, 1024], P(None, 'tp'), may hold values from -0.125 to 0.125
- value_weight: bfloat16 [2048, 1024], P(None, 'tp'), may hold values from -0.125 to 0.125
- output_weight: bfloat16 [1024, 2048], P(None, 'tp'), may hold values from -1.5 to 1.5
Outputs:
- attended: bfloat16 [8192, 2048], P(('grp', 'sp'), 'tp'), parts along dimension 0
There are 2 independent parts, one for each index of `grp`. A program takes and returns all parts, laid end to end along the dimension named above; an argument that names none is the same for every part. Nothing has to cross between parts.
All inputs are finite; a program needn't handle non-finite values.
Results may differ from a plain program's by a relative error of at most 0.012.
The roundings to bfloat16 on the way count: a program that leaves them out, or rounds other values in their place, can miss the bound.
Values may be sent and summed in bfloat16 or wider, within the bound.
A program may use at most 128 MiB of HBM per device.

v0:
```python
import jax
import jax.numpy as jnp
from jax import lax
from jax.sharding import PartitionSpec as P

HEAD = 128
REACH_STEPS = 128
MIDDLE_DILATION = 4
FAR_DILATION = 16


THETA_BASE = 500000.0


def passed_along(block, axis, distance):
    devices = range(lax.axis_size(axis))
    route = [(i - distance, i) for i in devices if i - distance in devices]
    return lax.ppermute(block, axis, route)


def rotate(values, positions):
    half = values.shape[-1] // 2
    inverse = THETA_BASE ** (-jnp.arange(half, dtype=jnp.float32) / half)
    angles = positions[:, None, None] * inverse
    cosine = jnp.cos(angles)
    sine = jnp.sin(angles)
    first = values[..., :half]
    second = values[..., half:]
    return jnp.concatenate(
        [first * cosine - second * sine, second * cosine + first * sine], axis=-1
    )


def windowed(queries, key_context, value_context, pattern_dilation, context_start):
    query_rows, heads, size = queries.shape
    sub_length = query_rows // pattern_dilation
    if sub_length >= REACH_STEPS:
        blocks = sub_length // REACH_STEPS
        block_rows = REACH_STEPS
        query_blocks = queries.reshape(blocks, REACH_STEPS, pattern_dilation, heads, size)

        def arrange(array):
            whole = array.reshape(blocks + 1, REACH_STEPS, pattern_dilation, heads, size)
            return jnp.concatenate([whole[:-1], whole[1:]], axis=1)

    else:
        blocks = 1
        block_rows = sub_length
        query_blocks = queries.reshape(1, sub_length, pattern_dilation, heads, size)

        def arrange(array):
            return array.reshape(1, sub_length + REACH_STEPS, pattern_dilation, heads, size)

    key_blocks = arrange(key_context)
    value_blocks = arrange(value_context)
    scores = jnp.einsum(
        "nqrhd,nkrhd->nrhqk", query_blocks, key_blocks, preferred_element_type=jnp.float32
    ) * HEAD ** (-0.5)
    query_index = jnp.arange(block_rows)[:, None] + REACH_STEPS
    key_index = jnp.arange(block_rows + REACH_STEPS)[None, :]
    distance = query_index - key_index
    sub_index = (
        jnp.arange(blocks)[:, None] * block_rows + jnp.arange(block_rows + REACH_STEPS)[None, :]
    )
    key_position = (
        context_start
        + sub_index[:, None, :] * pattern_dilation
        + jnp.arange(pattern_dilation)[None, :, None]
    )
    allowed = ((distance >= 0) & (distance <= REACH_STEPS))[None, None, None] & (key_position >= 0)[
        :, :, None, None, :
    ]
    scores = jnp.where(allowed, scores, -jnp.inf)
    top = jnp.max(scores, axis=-1, keepdims=True)
    offset_keys = jnp.exp(scores - top)
    total = jnp.sum(offset_keys, axis=-1, keepdims=True)
    weights = (offset_keys / total).astype(jnp.bfloat16)
    result = jnp.einsum(
        "nrhqk,nkrhd->nqrhd", weights, value_blocks, preferred_element_type=jnp.float32
    ).reshape(query_rows, heads, size)
    lse = jnp.transpose((top + jnp.log(total))[..., 0], (0, 3, 1, 2)).reshape(query_rows, heads)
    return (result, lse)


def body(tokens, query_weight, key_weight, value_weight, output_weight):
    width = query_weight.shape[1]
    heads = width // HEAD
    piece = lax.all_gather(tokens, "tp", axis=0, tiled=True)
    projected = jnp.stack(
        [
            jnp.dot(piece, query_weight, preferred_element_type=jnp.float32),
            jnp.dot(piece, key_weight, preferred_element_type=jnp.float32),
            jnp.dot(piece, value_weight, preferred_element_type=jnp.float32),
        ]
    )
    query_rows = projected.shape[1]
    offset = lax.axis_index("sp") * query_rows
    positions = (offset + jnp.arange(query_rows, dtype=jnp.int32)).astype(jnp.float32)
    queries = rotate(projected[0].reshape(query_rows, heads, HEAD), positions).astype(jnp.bfloat16)
    keys = rotate(projected[1].reshape(query_rows, heads, HEAD), positions).astype(jnp.bfloat16)
    values = projected[2].astype(jnp.bfloat16).reshape(query_rows, heads, HEAD)
    matched_pairs = jnp.stack([keys, values])
    reach_extent = -(-(FAR_DILATION * REACH_STEPS) // query_rows)
    context = matched_pairs
    holding = 1
    while holding < reach_extent + 1:
        count = min(holding, reach_extent + 1 - holding)
        newest = context[:, context.shape[1] - count * query_rows :]
        received = passed_along(newest, "sp", holding)
        context = jnp.concatenate([received, context], axis=1)
        holding = holding + count
    context_length = context.shape[1]
    results = []
    lses = []
    for pattern_dilation in (1, MIDDLE_DILATION, FAR_DILATION):
        reach_rows = pattern_dilation * REACH_STEPS
        window = context[:, context_length - query_rows - reach_rows :]
        result, lse = windowed(queries, window[0], window[1], pattern_dilation, offset - reach_rows)
        results.append(result)
        lses.append(lse)
    mixing = jax.nn.softmax(jnp.stack(lses, axis=0), axis=0)
    mixed = jnp.sum(mixing[..., None] * jnp.stack(results, axis=0), axis=0)
    mixed = mixed.astype(jnp.bfloat16).reshape(query_rows, width)
    attended = jnp.dot(
        lax.all_gather(mixed, "tp", axis=1, tiled=True),
        output_weight,
        preferred_element_type=jnp.float32,
    )
    return attended.astype(jnp.bfloat16)


def solution(mesh):
    in_specs = (
        P(("grp", "sp", "tp"), None),
        P(None, "tp"),
        P(None, "tp"),
        P(None, "tp"),
        P(None, "tp"),
    )
    out_specs = P(("grp", "sp"), "tp")
    return jax.shard_map(body, mesh=mesh, in_specs=in_specs, out_specs=out_specs, check_vma=False)
```

profile of v0, /device:TPU:19, one launch (start us, length us, event | category | flops | bytes accessed | tf_op | source)
XLA Modules:
  0.0 201.0 jit_solution(4947704851931204526)
XLA Ops:
  7.5 1.7 multiply_cosine_fusion
  9.2 12.0 %all-gather.3.cloned.1.call-done = bf16[512,2048]{1,0:T(8,128)(2,1)} async-done(((bf16[256,2048]{1,0:T(8,128)(2,1)}), bf16[512,2048]{1,0:T(8,128)(2,1)}) %all-gather.3.cloned.1.call-update) | async-done | bytes 2097168 | tf_op jit(solution)/shard_map/all_gather | solution.py:88
  21.3 3.5 %convolution_convert_fusion.1 = bf16[512,512]{0,1:T(8,128)(2,1)S(1)} fusion(bf16[512,2048]{1,0:T(8,128)(2,1)} %all-gather.3.cloned.1.call-done, bf16[2048,512]{1,0:T(8,128)(2,1)} %param.8), kind=kOutput, calls=%fused_computation.27 | convolution fusion | flops 1074003968 | bytes 4718592 | tf_op jit(solution)/shard_map/dot_general | solution.py:93
  24.8 1.0 copy.86
  25.8 3.7 %fusion.66 = f32[512,512]{0,1:T(8,128)S(1)} fusion(bf16[512,2048]{1,0:T(8,128)(2,1)} %all-gather.3.cloned.1.call-done, bf16[2048,512]{1,0:T(8,128)(2,1)} %param.7), kind=kOutput, calls=%fused_computation.113 | convolution fusion | flops 1073741824 | bytes 5242880 | tf_op jit(solution)/shard_map/dot_general | solution.py:92
  29.6 1.5 copy-done.24
  31.1 1.3 fusion.65
  32.4 1.1 fusion.63
  33.5 2.4 %copy.126 = f32[512,4,64]{2,0,1:T(8,128)} copy(f32[512,4,64]{0,2,1:T(8,128)} %get-tuple-element.15) | data formatting | bytes 1048576
  35.8 1.3 copy.128
  37.1 2.4 %copy.125 = f32[512,4,64]{2,0,1:T(8,128)} copy(f32[512,4,64]{0,2,1:T(8,128)} %get-tuple-element.16) | data formatting | bytes 1048576
  39.5 1.3 copy.127
  40.8 3.8 %subtract_convert_fusion.1 = (bf16[512,4,64]{2,0,1:T(8,128)(2,1)}, bf16[512,4,64]{2,0,1:T(8,128)(2,1)}, bf16[512,4,64]{2,0,1:T(8,128)(2,1)S(1)}, bf16[512,4,64]{2,0,1:T(8,128)(2,1)S(1)}) fusion(f32[512,4,64]{2,0,1:T(8,128)} %copy.126, f32[512,4,64]{2,0,1:T(8,128)} %copy.125, f32[512,64]{1,0:T(8,128)} %get-tuple-element.24, ...), kind=kLoop, calls=%fused_computation.52 | loop fusion | flops 2097152 | bytes 3407872 | tf_op jit(solution)/shard_map/convert.23
  44.7 1.3 pad_maximum_fusion
  45.9 3.1 %collective-permute-start = (bf16[2,512,4,128]{3,1,2,0:T(8,128)(2,1)}, bf16[2,512,4,128]{3,1,2,0:T(8,128)(2,1)}, u32[]{:S(2)}, u32[]{:S(2)}) collective-permute-start(bf16[2,512,4,128]{3,1,2,0:T(8,128)(2,1)} %pad_maximum_fusion), channel_id=1, source_target_pairs={{0,2},{2,4},{4,6},{6,8},{8,10},{10,12},{12,14},{1,3},{3,5},{5,7},{... | collective-permute-start | bytes 3145736 | tf_op jit(solution)/shard_map/ppermute | solution.py:18
  49.5 2.1 %copy.107 = bf16[512,512]{1,0:T(8,128)(2,1)} copy(bf16[512,512]{0,1:T(8,128)(2,1)} %copy-done.5) | data formatting | bytes 1048576 | tf_op jit(solution)/shard_map/convert_element_type | solution.py:101
  51.6 2.0 slice.86
  53.6 1.3 collective-permute-start.1
  54.9 2.1 %copy.105 = bf16[4,128,1,4,128]{4,1,3,0,2:T(8,128)(2,1)} copy(bf16[4,128,1,4,128]{1,0,4,3,2:T(4,128)(2,1)} %slice.86) | data formatting | bytes 1048576 | tf_op jit(solution)/shard_map/slice | solution.py:44
  57.0 2.0 slice.89
  59.0 2.1 %copy.109 = bf16[1,128,4,4,128]{4,1,3,2,0:T(8,128)(2,1)} copy(bf16[1,128,4,4,128]{4,3,2,1,0:T(4,128)(2,1)} %slice.89) | data formatting | bytes 1048576 | tf_op jit(solution)/shard_map/slice | solution.py:44
  61.4 0.9 copy.99
  62.4 0.9 copy.98
  63.3 10.2 %collective-permute-done = bf16[2,512,4,128]{3,1,2,0:T(8,128)(2,1)} collective-permute-done((bf16[2,512,4,128]{3,1,2,0:T(8,128)(2,1)}, bf16[2,512,4,128]{3,1,2,0:T(8,128)(2,1)}, u32[]{:S(2)}, u32[]{:S(2)}) %collective-permute-start) | collective-permute-done | bytes 1048608 | tf_op jit(solution)/shard_map/ppermute | solution.py:18
  73.6 2.9 %maximum_maximum_fusion.1 = bf16[2,1024,4,128]{3,1,2,0:T(8,128)(2,1)} fusion(bf16[1,512,4,128]{3,1,2,0:T(8,128)(2,1)S(1)} %copy-done.3, bf16[1,512,4,64]{3,1,2,0:T(8,128)(2,1)S(1)} %bitcast.100, bf16[1,512,4,64]{3,1,2,0:T(8,128)(2,1)S(1)} %bitcast.105, bf16[2,512,4,128]{3,1,2,0:T(8,128)(2,1)} %collective-permute-done), kind=kLoop, calls=%fused_computation.7 | loop fusion | flops 8388608 | bytes 4194304 | tf_op jit(solution)/shard_map/concatenate | solution.py:110
  76.5 2.1 %fusion.61 = (bf16[1,512,4,128]{3,1,2,0:T(8,128)(2,1)S(1)}, bf16[1,512,4,128]{3,1,2,0:T(8,128)(2,1)}) fusion(bf16[2,1024,4,128]{3,1,2,0:T(8,128)(2,1)} %maximum_maximum_fusion.1), kind=kLoop, calls=%fused_computation.108 | loop fusion | bytes 2097152 | tf_op jit(solution)/shard_map/slice | solution.py:44
  78.5 3.2 %collective-permute-start.2 = (bf16[2,1024,4,128]{3,1,2,0:T(8,128)(2,1)}, bf16[2,1024,4,128]{3,1,2,0:T(8,128)(2,1)}, u32[]{:S(2)}, u32[]{:S(2)}) collective-permute-start(bf16[2,1024,4,128]{3,1,2,0:T(8,128)(2,1)} %maximum_maximum_fusion.1), channel_id=1, source_target_pairs={{0,4},{2,6},{4,8},{6,10},{8,12},{10,14},{1,5},{3,7},{5,9},{7,11},{... | collective-permute-start | bytes 6291464 | tf_op jit(solution)/shard_map/ppermute | solution.py:18
  81.8 2.1 %fusion.62 = (bf16[1,512,4,128]{3,1,2,0:T(8,128)(2,1)S(1)}, bf16[1,512,4,128]{3,1,2,0:T(8,128)(2,1)}) fusion(bf16[2,512,4,128]{3,1,2,0:T(8,128)(2,1)} %collective-permute-done), kind=kLoop, calls=%fused_computation.109 | loop fusion | bytes 2097152 | tf_op jit(solution)/shard_map/slice | solution.py:44
  84.0 1.2 fusion.5
  85.2 1.2 fusion.6
  86.5 1.6 fusion.8
  89.3 0.8 copy.97
  91.7 1.1 copy.108
  92.9 2.6 %convolution_bitcast_fusion = f32[1,128,4,4,128]{4,1,3,2,0:T(8,128)S(1)} fusion(bf16[1,128,4,4,128]{4,1,3,2,0:T(8,128)(2,1)} %copy.109, bf16[1,128,4,4,128]{4,1,3,2,0:T(8,128)(2,1)S(1)} %copy.108, f32[4,4,128,256]{3,2,1,0:T(8,128)} %copy-done.14, f32[4,4,128]{2,1,0:T(4,128)} %copy-done.22, f32[4,4,128]{2,1,0:T(4,128)} %copy-done.21, ...), kind=kOutput, calls=%fused_computation.25 | convolution fusion | flops 138936320 | bytes 4341760 | tf_op jit(solution)/shard_map/nrhqk,nkrhd->nqrhd/dot_general | solution.py:78
  95.5 1.6 copy.110
  97.2 1.4 convolution_bitcast_fusion.1
  98.6 1.1 copy.106
  99.7 46.3 %collective-permute-done.2 = bf16[2,1024,4,128]{3,1,2,0:T(8,128)(2,1)} collective-permute-done((bf16[2,1024,4,128]{3,1,2,0:T(8,128)(2,1)}, bf16[2,1024,4,128]{3,1,2,0:T(8,128)(2,1)}, u32[]{:S(2)}, u32[]{:S(2)}) %collective-permute-start.2) | collective-permute-done | bytes 2097184 | tf_op jit(solution)/shard_map/ppermute | solution.py:18
  146.0 3.5 %maximum_maximum_fusion = bf16[2,2560,4,128]{3,1,2,0:T(8,128)(2,1)S(1)} fusion(bf16[1,512,4,128]{3,1,2,0:T(8,128)(2,1)S(1)} %copy-done.4, bf16[1,512,4,64]{3,1,2,0:T(8,128)(2,1)S(1)} %bitcast.102, bf16[1,512,4,64]{3,1,2,0:T(8,128)(2,1)S(1)} %bitcast.107, bf16[2,512,4,128]{3,1,2,0:T(8,128)(2,1)} %collective-permute-done, ...), kind=kLoop, calls=%fused_computation | loop fusion | flops 31457280 | bytes 10485760 | tf_op jit(solution)/shard_map/concatenate | solution.py:110
  149.5 1.8 fusion.60
  151.3 2.0 %fusion.7 = (f32[16,4,32]{2,1,0:T(4,128)S(1)}, f32[16,4,32,160]{3,2,1,0:T(8,128)S(1)}) fusion(pred[16,32,160]{2,1,0:T(8,128)(4,1)S(1)} %broadcast_and_fusion, bf16[160,16,4,128]{3,1,0,2:T(8,128)(2,1)S(1)} %bitcast.108, bf16[32,16,4,64]{3,0,2,1:T(8,128)(2,1)S(1)} %copy-done.10, bf16[32,16,4,64]{3,0,2,1:T(8,128)(2,1)S(1)} %copy-done.11), kind=kOutput, calls=%fused_computation.19 | convolution fusion | flops 85915648 | bytes 4546560 | tf_op jit(solution)/shard_map/nqrhd,nkrhd->nrhqk/dot_general | solution.py:56
  153.4 1.4 copy-done.1
  154.7 1.0 fusion.10
  156.0 4.1 %fusion.11 = f32[1,32,16,4,128]{4,1,3,2,0:T(8,128)S(1)} fusion(bf16[160,16,4,128]{3,1,0,2:T(8,128)(2,1)} %bitcast.119, f32[16,4,32,160]{3,2,1,0:T(8,128)} %copy-done.1, f32[16,4,32]{2,1,0:T(4,128)S(1)} %fusion.10, f32[16,4,32]{2,1,0:T(4,128)S(1)} %get-tuple-element.25, pred[16,32,160]{2,1,0:T(8,128)(4,1)S(1)} %broadcast_and_fusion), kind=kOutput, calls=%fused_computation.24 | convolution fusion | flops 85524480 | bytes 5079040 | tf_op jit(solution)/shard_map/nrhqk,nkrhd->nqrhd/dot_general | solution.py:78
  161.7 1.1 fusion
  162.8 1.0 copy.113
  163.9 26.9 %all-gather.5.cloned.1.call-done = bf16[512,1024]{0,1:T(8,128)(2,1)} async-done(((bf16[512,512]{0,1:T(8,128)(2,1)}), bf16[512,1024]{0,1:T(8,128)(2,1)}) %all-gather.5.cloned.1.call-update) | async-done | bytes 1048592 | tf_op jit(solution)/shard_map/all_gather | solution.py:125
  190.7 3.5 %convolution_convert_fusion = bf16[512,1024]{1,0:T(8,128)(2,1)} fusion(bf16[512,1024]{0,1:T(8,128)(2,1)} %all-gather.5.cloned.1.call-done, bf16[1024,1024]{1,0:T(8,128)(2,1)S(1)} %copy-done), kind=kOutput, calls=%fused_computation.23 | convolution fusion | flops 1074266112 | bytes 4194304 | tf_op jit(solution)/shard_map/dot_general | solution.py:124
  (87 shorter events, 6.6 us)
Async XLA Ops:
  6.5 184.2 %copy-start = (bf16[1024,1024]{1,0:T(8,128)(2,1)S(1)}, bf16[1024,1024]{1,0:T(8,128)(2,1)}, u32[]{:S(2)}) copy-start(bf16[1024,1024]{1,0:T(8,128)(2,1)} %param.9) | copy-start | bytes 6291460
  6.5 14.7 %all-gather.3.cloned.1.call-start = ((), (), s32[]{:S(2)}) async-start(), calls=%async_computation | async-start | bytes 3145728 | tf_op jit(solution)/shard_map/all_gather | solution.py:88
  7.3 183.5 %all-gather.5.cloned.1.call-start = ((), (), s32[]{:S(2)}) async-start(), calls=%async_computation.1 | async-start | bytes 1572864 | tf_op jit(solution)/shard_map/all_gather | solution.py:125
  24.8 4.7 %copy-start.5 = (bf16[512,512]{0,1:T(8,128)(2,1)}, bf16[512,512]{0,1:T(8,128)(2,1)S(1)}, u32[]{:S(2)}) copy-start(bf16[512,512]{0,1:T(8,128)(2,1)S(1)} %convolution_convert_fusion.1) | copy-start | bytes 1572868
  25.8 3.8 %copy-start.25 = (bf16[512,2048]{1,0:T(8,128)(2,1)S(1)}, bf16[512,2048]{1,0:T(8,128)(2,1)}, u32[]{:S(2)}) copy-start(bf16[512,2048]{1,0:T(8,128)(2,1)} %all-gather.3.cloned.1.call-done) | copy-start | bytes 6291460
  29.5 1.6 copy-start.24
  40.8 3.8 %copy-start.2 = (bf16[1,512,4,128]{3,1,2,0:T(8,128)(2,1)S(1)}, bf16[1,512,4,128]{3,1,2,0:T(8,128)(2,1)}, u32[]{:S(2)}) copy-start(bf16[1,512,4,128]{3,1,2,0:T(8,128)(2,1)} %copy.86) | copy-start | bytes 1572868
  45.9 27.6 %collective-permute-start = (bf16[2,512,4,128]{3,1,2,0:T(8,128)(2,1)}, bf16[2,512,4,128]{3,1,2,0:T(8,128)(2,1)}, u32[]{:S(2)}, u32[]{:S(2)}) collective-permute-start(bf16[2,512,4,128]{3,1,2,0:T(8,128)(2,1)} %pad_maximum_fusion), channel_id=1, source_target_pairs={{0,2},{2,4},{4,6},{6,8},{8,10},{10,12},{12,14},{1,3},{3,5},{5,7},{... | collective-permute-start | bytes 3145736 | tf_op jit(solution)/shard_map/ppermute | solution.py:18
  49.5 36.9 %copy-start.15 = (pred[4,128,256]{2,1,0:T(8,128)(4,1)}, pred[4,128,256]{2,1,0:T(8,128)(4,1)S(1)}, u32[]{:S(2)}) copy-start(pred[4,128,256]{2,1,0:T(8,128)(4,1)S(1)} %get-tuple-element.21) | copy-start | bytes 393220
  49.5 36.9 %copy-start.17 = (pred[4,128,256]{2,1,0:T(8,128)(4,1)}, pred[4,128,256]{2,1,0:T(8,128)(4,1)S(1)}, u32[]{:S(2)}) copy-start(pred[4,128,256]{2,1,0:T(8,128)(4,1)S(1)} %get-tuple-element.22) | copy-start | bytes 393220
  53.6 46.1 %collective-permute-start.1 = (bf16[2,512,4,128]{3,1,2,0:T(8,128)(2,1)}, bf16[2,512,4,128]{3,1,2,0:T(8,128)(2,1)}, u32[]{:S(2)}, u32[]{:S(2)}) collective-permute-start(bf16[2,512,4,128]{3,1,2,0:T(8,128)(2,1)} %pad_maximum_fusion), channel_id=1, source_target_pairs={{0,8},{2,10},{4,12},{6,14},{1,9},{3,11},{5,13},{7,15},{16,24},{18,... | collective-permute-start | bytes 3145736 | tf_op jit(solution)/shard_map/ppermute | solution.py:18
  59.0 2.3 %copy-start.7 = (bf16[512,4,64]{2,0,1:T(8,128)(2,1)S(1)}, bf16[512,4,64]{2,0,1:T(8,128)(2,1)}, u32[]{:S(2)}) copy-start(bf16[512,4,64]{2,0,1:T(8,128)(2,1)} %get-tuple-element.8) | copy-start | bytes 786436
  61.0 1.3 copy-start.6
  61.3 12.3 %copy-start.3 = (bf16[1,512,4,128]{3,1,2,0:T(8,128)(2,1)S(1)}, bf16[1,512,4,128]{3,1,2,0:T(8,128)(2,1)}, u32[]{:S(2)}) copy-start(bf16[1,512,4,128]{3,1,2,0:T(8,128)(2,1)} %copy.86) | copy-start | bytes 1572868
  78.5 67.5 %collective-permute-start.2 = (bf16[2,1024,4,128]{3,1,2,0:T(8,128)(2,1)}, bf16[2,1024,4,128]{3,1,2,0:T(8,128)(2,1)}, u32[]{:S(2)}, u32[]{:S(2)}) collective-permute-start(bf16[2,1024,4,128]{3,1,2,0:T(8,128)(2,1)} %maximum_maximum_fusion.1), channel_id=1, source_target_pairs={{0,4},{2,6},{4,8},{6,10},{8,12},{10,14},{1,5},{3,7},{5,9},{7,11},{... | collective-permute-start | bytes 6291464 | tf_op jit(solution)/shard_map/ppermute | solution.py:18
  85.2 1.3 copy-start.12
  86.4 1.8 copy-start.14
  86.4 1.8 copy-start.21
  88.1 0.6 copy-start.22
  92.9 4.3 %copy-start.16 = (pred[4,128,256]{2,1,0:T(8,128)(4,1)S(1)}, pred[4,128,256]{2,1,0:T(8,128)(4,1)}, u32[]{:S(2)}) copy-start(pred[4,128,256]{2,1,0:T(8,128)(4,1)} %copy-done.15) | copy-start | bytes 393220
  92.9 4.3 %copy-start.18 = (bf16[4,128,1,4,128]{4,1,3,0,2:T(8,128)(2,1)S(1)}, bf16[4,128,1,4,128]{4,1,3,0,2:T(8,128)(2,1)}, u32[]{:S(2)}) copy-start(bf16[4,128,1,4,128]{4,1,3,0,2:T(8,128)(2,1)} %copy.105) | copy-start | bytes 1572868
  92.9 4.3 %copy-start.19 = (bf16[1,512,4,128]{3,1,2,0:T(8,128)(2,1)S(1)}, bf16[1,512,4,128]{3,1,2,0:T(8,128)(2,1)}, u32[]{:S(2)}) copy-start(bf16[1,512,4,128]{3,1,2,0:T(8,128)(2,1)} %get-tuple-element.12) | copy-start | bytes 1572868
  95.5 1.7 copy-start.13
  98.6 47.4 %copy-start.4 = (bf16[1,512,4,128]{3,1,2,0:T(8,128)(2,1)S(1)}, bf16[1,512,4,128]{3,1,2,0:T(8,128)(2,1)}, u32[]{:S(2)}) copy-start(bf16[1,512,4,128]{3,1,2,0:T(8,128)(2,1)} %copy.86) | copy-start | bytes 1572868
  149.5 1.9 copy-start.10
  149.5 1.8 copy-start.11
  153.4 1.4 copy-start.1
  156.0 4.8 %copy-start.23 = (f32[512,4]{0,1:T(4,128)S(1)}, f32[512,4]{0,1:T(4,128)}, u32[]{:S(2)}) copy-start(f32[512,4]{0,1:T(4,128)} %stack_reshape.23) | copy-start | bytes 24580
  160.1 0.7 copy-start.20
  160.2 1.2 copy-start.8
  160.2 1.6 copy-start.9
Sparse Core Ops, SparseCore 0:
  8.9 12.3 all-gather.2
  164.0 26.7 all-gather.4
where the time goes:
time: 203 us; the launch traced here: 201 us
  waiting for transfers between devices  96.1 us (47%)
  local copies, waits for them, and re-layouts  40.8 us (20%)
  matrix products  24.4 us (12%)
  other arithmetic  18.1 us (9%)
  between operations  14 us (7%)
  starting transfers between devices  7.66 us (4%)
    ppermute x3, waiting for transfers between devices, passed_along(): return lax.ppermute(block, axis, route)  56.5 us
    all_gather x1, waiting for transfers between devices, body(): lax.all_gather(mixed, 'tp', axis=1, tiled=True)  26.9 us
    slice x8, local copies, waits for them, and re-layouts, arrange(): return jnp.concatenate([whole[:-1], whole[1:]], axis=1)  13.5 us
    all_gather x1, waiting for transfers between devices, body(): piece = lax.all_gather(tokens, 'tp', axis=0, tiled=True)  12 us
    unnamed x56, local copies, waits for them, and re-layouts  11.8 us
    dot_general x3, matrix products, windowed(): jnp.einsum('nrhqk,nkrhd->nqrhd', weights, value_blocks, preferred_element...  8.08 us
    ppermute x3, starting transfers between devices, passed_along(): return lax.ppermute(block, axis, route)  7.62 us
    concatenate x2, other arithmetic, body(): context = jnp.concatenate([received, context], axis=1)  6.37 us
  transfers between devices with their start and end apart: 5, of which 4 were waited for; matrix products, arithmetic and copies ran while one was open for 18% of the time, Pallas kernels for 0%

commit v1 on v0

v1 whole, which is shorter than its diff:
```python
import functools

import jax
import jax.numpy as jnp
from jax import lax
from jax.experimental import pallas as pl
from jax.experimental.pallas import tpu as pltpu
from jax.sharding import PartitionSpec as P

HEAD = 128
REACH_STEPS = 128
MIDDLE_DILATION = 4
FAR_DILATION = 16
THETA_BASE = 500000.0
NEG = -1e30
MESH = pl.DeviceIdType.MESH
F32 = jnp.float32
BF16 = jnp.bfloat16

B, D, A, C, O = 0, 1, 2, 3, 4
SLOTS = 5
CLASSES = MIDDLE_DILATION
CLASS_ROWS = 128


def spot(i):
    return (i >> 6) * 256 + (i & 15) * 16 + ((i >> 4) & 3) * 4


def iota(shape, dim):
    return lax.broadcasted_iota(jnp.int32, shape, dim)


def rotated(x, cosine, sine):
    return x * cosine + pltpu.roll(x, HEAD // 2, 1) * sine


def softmax(scores, values):
    top = jnp.max(scores, axis=-1, keepdims=True)
    raised = jnp.exp(scores - top)
    total = jnp.sum(raised, axis=-1, keepdims=True)
    weights = (raised * (1.0 / total)).astype(BF16)
    result = jnp.dot(weights, values, preferred_element_type=F32)
    return result, top + jnp.log(total)


def transposed_dot(a, b):
    return lax.dot_general(a, b, (((1,), (1,)), ((), ())), preferred_element_type=F32)


def kernel(
    n_sp, heads,
    tok_hbm, wq_hbm, wk_hbm, wv_hbm, wo_hbm, cos_ref, sin_ref,
    out_ref,
    tok, wkv, wq, wo, xg, ctx, q, k1, v1, perm, unperm, b16, b4, b1, mixp, mixg,
    load_sem, x_sem, ctx_send, ctx_recv, mix_send, mix_recv,
):
    sp = lax.axis_index("sp")
    tp = lax.axis_index("tp")
    z = sp // 2
    odd = sp % 2
    even = odd == 0
    other = 1 - tp
    has_next = z + 1 < n_sp // 2

    tok_copy = pltpu.make_async_copy(tok_hbm, tok, load_sem.at[0])
    tok_copy.start()
    kv_copies = []
    for h in range(heads):
        cols = pl.ds(h * HEAD, HEAD)
        pair = (
            pltpu.make_async_copy(wk_hbm.at[:, cols], wkv.at[h, :, pl.ds(0, HEAD)], load_sem.at[1 + 2 * h]),
            pltpu.make_async_copy(wv_hbm.at[:, cols], wkv.at[h, :, pl.ds(HEAD, HEAD)], load_sem.at[2 + 2 * h]),
        )
        for copy in pair:
            copy.start()
        kv_copies.append(pair)
    q_copies = []
    for p in range(heads // 2):
        copy = pltpu.make_async_copy(
            wq_hbm.at[:, pl.ds(p * 2 * HEAD, 2 * HEAD)], wq.at[p], load_sem.at[1 + 2 * heads + p])
        copy.start()
        q_copies.append(copy)
    wo_copy = pltpu.make_async_copy(wo_hbm, wo, load_sem.at[1 + 2 * heads + heads // 2])
    wo_copy.start()

    barrier = pltpu.get_barrier_semaphore()
    y_partner = sp + 1 - 2 * odd

    def greet(ids):
        pl.semaphore_signal(barrier, inc=1, device_id=ids, device_id_type=MESH)

    greet({"tp": other})
    greet({"sp": y_partner})

    @pl.when(has_next)
    def _():
        greet({"sp": sp + 2})

    @pl.when(z > 0)
    def _():
        greet({"sp": sp - 2})

    row = iota((256, 256), 0)
    perm[...] = jnp.where(spot(row & 63) + (row >> 6) == iota((256, 256), 1), 1.0, 0.0).astype(BF16)

    pl.semaphore_wait(barrier, 2 + has_next.astype(jnp.int32) + (z > 0).astype(jnp.int32))

    tok_copy.wait()
    width = tok.shape[1]

    def reorder(i, _):
        cols = pl.ds(pl.multiple_of(i * 512, 512), 512)
        moved = jnp.dot(perm[...], tok[:, cols], preferred_element_type=F32).astype(BF16)
        xg[:, tp, :, cols] = moved.reshape(CLASSES, 64, 512)
        return 0

    lax.fori_loop(0, width // 512, reorder, 0)
    x_copy = pltpu.make_async_remote_copy(
        src_ref=xg.at[:, tp], dst_ref=xg.at[:, tp], send_sem=x_sem.at[0], recv_sem=x_sem.at[1],
        device_id={"tp": other}, device_id_type=MESH)
    x_copy.start()

    qi, kj = iota((128, 640), 0), iota((128, 640), 1)
    dist = 4 - (kj >> 7)
    diff = spot(qi) - spot(kj & 127) + 512 * dist
    here = dist <= sp
    far = here & ((diff & 15) == 0) & (diff >= 0) & (diff <= FAR_DILATION * REACH_STEPS)
    b16[...] = jnp.where(far, 0.0, NEG)
    mid = here & (diff >= 0) & (diff <= MIDDLE_DILATION * REACH_STEPS)
    b4[...] = jnp.where(mid, 0.0, NEG)[:, 384:]
    key_spot = jnp.where(kj < 128, kj - 128, spot(kj & 127) + ((kj >> 7) - 1))
    for c in range(CLASSES):
        near = spot(qi) + c - key_spot
        ok = (near >= 0) & (near <= REACH_STEPS) & ((kj >= 128) | (sp > 0))
        b1[c] = jnp.where(ok, 0.0, NEG)
    col = iota((512, 512), 1)
    unperm[...] = jnp.where(spot(col & 127) + (col >> 7) == iota((512, 512), 0), 1.0, 0.0).astype(BF16)

    for slot in (B, D, A, C):
        @pl.when(sp < 4 - slot)
        def _():
            def clear(h, _):
                ctx[h, :, :, slot] = jnp.zeros((2, CLASSES, 128, HEAD), BF16)
                return 0
            lax.fori_loop(0, heads, clear, 0)

    def send(h, src, dst, ids):
        return pltpu.make_async_remote_copy(
            src_ref=ctx.at[h, :, :, src], dst_ref=ctx.at[h, :, :, dst],
            send_sem=ctx_send.at[dst, h], recv_sem=ctx_recv.at[dst, h],
            device_id=ids, device_id_type=MESH)

    down = {"sp": sp + 2}
    side = {"sp": y_partner}

    def sends_of(h, src):
        if src == O:
            return [(has_next, send(h, O, A, down)), (even, send(h, O, C, side))]
        if src == A:
            return [(has_next & (z > 0), send(h, A, B, down)),
                    (even & (z > 0), send(h, A, D, side)),
                    ((odd == 1) & (z > 0), send(h, A, C, side))]
        return [((odd == 1) & (z > 1), send(h, B, D, side))]

    def start_all(h, src):
        for condition, copy in sends_of(h, src):
            @pl.when(condition)
            def _():
                copy.start()

    def receive(h, slot):
        @pl.when(sp >= 4 - slot)
        def _():
            send(h, slot, slot, side).wait_recv()

    x_copy.wait_recv()

    def tokens():
        return xg[...].reshape(512, width)

    def project_kv(h, _):
        kv = jnp.dot(tokens(), wkv[h], preferred_element_type=F32)
        k = rotated(kv[:, :HEAD], cos_ref[...], sin_ref[...]).astype(BF16)
        ctx[h, 0, :, O] = k.reshape(CLASSES, 128, HEAD)
        ctx[h, 1, :, O] = kv[:, HEAD:].astype(BF16).reshape(CLASSES, 128, HEAD)
        start_all(h, O)
        return 0

    for pair in kv_copies:
        for copy in pair:
            copy.wait()
    lax.fori_loop(0, heads, project_kv, 0)

    for copy in q_copies:
        copy.wait()

    def project_q(p, _):
        qq = jnp.dot(tokens(), wq[p], preferred_element_type=F32)
        for s in range(2):
            r = rotated(qq[:, s * HEAD:(s + 1) * HEAD], cos_ref[...], sin_ref[...])
            q[2 * p + s] = r.astype(BF16).reshape(CLASSES, 128, HEAD)
        return 0

    lax.fori_loop(0, heads // 2, project_q, 0)

    def relay(h, _):
        receive(h, A)
        start_all(h, A)
        return 0

    lax.fori_loop(0, heads, relay, 0)

    def mix_copy(h):
        cols = pl.ds(pl.multiple_of(h * HEAD, HEAD), HEAD)
        return pltpu.make_async_remote_copy(
            src_ref=mixg.at[tp, :, cols], dst_ref=mixg.at[tp, :, cols],
            send_sem=mix_send.at[h], recv_sem=mix_recv.at[h],
            device_id={"tp": other}, device_id_type=MESH)

    def attend(h, _):
        receive(h, B)
        start_all(h, B)
        receive(h, C)
        receive(h, D)
        tail = unperm[384:512, :]
        for kv, near in ((0, k1), (1, v1)):
            last = ctx[h, kv, :, C].reshape(512, HEAD)
            near[0:128] = jnp.dot(tail, last, preferred_element_type=F32).astype(BF16)
            near[128:640] = ctx[h, kv, :, O].reshape(512, HEAD)

        def of_class(c, _):
            qc = q[h, c]
            keys = ctx[h, 0, c].reshape(SLOTS * 128, HEAD)
            vals = ctx[h, 1, c].reshape(SLOTS * 128, HEAD)
            scores = transposed_dot(qc, keys) * HEAD ** (-0.5)
            r16, l16 = softmax(scores + b16[...], vals)
            r4, l4 = softmax(scores[:, 384:] + b4[...], vals[384:])
            r1, l1 = softmax(transposed_dot(qc, k1[...]) * HEAD ** (-0.5) + b1[c], v1[...])
            most = jnp.maximum(jnp.maximum(l16, l4), l1)
            e16, e4, e1 = jnp.exp(l16 - most), jnp.exp(l4 - most), jnp.exp(l1 - most)
            share = 1.0 / (e16 + e4 + e1)
            mixed = r1 * (e1 * share) + r4 * (e4 * share) + r16 * (e16 * share)
            mixp[pl.ds(pl.multiple_of(c * 128, 128), 128), :] = mixed.astype(BF16)
            return 0

        lax.fori_loop(0, CLASSES, of_class, 0)
        natural = jnp.dot(unperm[...], mixp[...], preferred_element_type=F32).astype(BF16)
        cols = pl.ds(pl.multiple_of(h * HEAD, HEAD), HEAD)
        mixg[tp, :, cols] = natural
        mix_copy(h).start()
        return 0

    lax.fori_loop(0, heads, attend, 0)

    wo_copy.wait()

    def gathered(h, _):
        mix_copy(h).wait_recv()
        return 0

    lax.fori_loop(0, heads, gathered, 0)
    half = mixg.shape[2]

    def project_out(i, _):
        cols = pl.ds(pl.multiple_of(i * 256, 256), 256)
        total = jnp.dot(mixg[0], wo[:half, cols], preferred_element_type=F32)
        total = total + jnp.dot(mixg[1], wo[half:, cols], preferred_element_type=F32)
        out_ref[:, cols] = total.astype(BF16)
        return 0

    lax.fori_loop(0, out_ref.shape[1] // 256, project_out, 0)

    x_copy.wait_send()

    def left(h, _):
        for src in (O, A, B):
            for condition, copy in sends_of(h, src):
                @pl.when(condition)
                def _():
                    copy.wait_send()
        mix_copy(h).wait_send()
        return 0

    lax.fori_loop(0, heads, left, 0)


def body(tokens, query_weight, key_weight, value_weight, output_weight):
    n_sp = lax.axis_size("sp")
    half_rows, width = tokens.shape
    rows = half_rows * lax.axis_size("tp")
    heads = query_weight.shape[1] // HEAD
    assert rows * 4 == FAR_DILATION * REACH_STEPS and rows == 512
    assert n_sp % 2 == 0 and lax.axis_size("tp") == 2 and heads % 2 == 0

    index = jnp.arange(rows, dtype=jnp.int32)
    positions = lax.axis_index("sp") * rows + spot(index & 127) + (index >> 7)
    half = HEAD // 2
    inverse = THETA_BASE ** (-jnp.arange(half, dtype=F32) / half)
    angles = positions.astype(F32)[:, None] * inverse
    cosine, sine = jnp.cos(angles), jnp.sin(angles)
    cos_table = jnp.concatenate([cosine, cosine], axis=1)
    sin_table = jnp.concatenate([-sine, sine], axis=1)

    anywhere = pl.BlockSpec(memory_space=pl.ANY)
    vmem = pl.BlockSpec(memory_space=pltpu.VMEM)
    out_cols = output_weight.shape[1]
    return pl.pallas_call(
        functools.partial(kernel, n_sp, heads),
        out_shape=jax.ShapeDtypeStruct((rows, out_cols), BF16),
        in_specs=[anywhere] * 5 + [vmem] * 2,
        out_specs=vmem,
        scratch_shapes=[
            pltpu.VMEM((half_rows, width), BF16),
            pltpu.VMEM((heads, width, 2 * HEAD), BF16),
            pltpu.VMEM((heads // 2, width, 2 * HEAD), BF16),
            pltpu.VMEM(output_weight.shape, BF16),
            pltpu.VMEM((CLASSES, 2, 64, width), BF16),
            pltpu.VMEM((heads, 2, CLASSES, SLOTS, 128, HEAD), BF16),
            pltpu.VMEM((heads, CLASSES, 128, HEAD), BF16),
            pltpu.VMEM((640, HEAD), BF16),
            pltpu.VMEM((640, HEAD), BF16),
            pltpu.VMEM((256, 256), BF16),
            pltpu.VMEM((512, 512), BF16),
            pltpu.VMEM((128, 640), F32),
            pltpu.VMEM((128, 256), F32),
            pltpu.VMEM((CLASSES, 128, 640), F32),
            pltpu.VMEM((512, HEAD), BF16),
            pltpu.VMEM((2, rows, heads * HEAD), BF16),
            pltpu.SemaphoreType.DMA((2 + 2 * heads + heads // 2,)),
            pltpu.SemaphoreType.DMA((2,)),
            pltpu.SemaphoreType.DMA((4, heads)),
            pltpu.SemaphoreType.DMA((4, heads)),
            pltpu.SemaphoreType.DMA((heads,)),
            pltpu.SemaphoreType.DMA((heads,)),
        ],
        compiler_params=pltpu.CompilerParams(
            collective_id=0, has_side_effects=True, vmem_limit_bytes=48 * 1024 * 1024
        ),
    )(tokens, query_weight, key_weight, value_weight, output_weight, cos_table, sin_table)


def solution(mesh):
    in_specs = (
        P(("grp", "sp", "tp"), None),
        P(None, "tp"),
        P(None, "tp"),
        P(None, "tp"),
        P(None, "tp"),
    )
    out_specs = P(("grp", "sp"), "tp")
    return jax.shard_map(body, mesh=mesh, in_specs=in_specs, out_specs=out_specs, check_vma=False)
```

time: 203 us -> 73.1 us (0.36)
  waiting for transfers between devices: 96.1 us -> 0 us
  Pallas kernels: 0 us -> 69.1 us
  local copies, waits for them, and re-layouts: 40.8 us -> 2.55 us
  matrix products: 24.4 us -> 0 us
  other arithmetic: 18.1 us -> 1.22 us
  between operations: 14 us -> 0.03 us
  starting transfers between devices: 7.66 us -> 0 us
    pallas_call x0 -> x1, Pallas kernels: none -> 69.1 us  [body(): pl.pallas_call(functools.partial(kernel, n_sp, heads), out_shape=jax.Shap...]
    ppermute x3 -> x0, waiting for transfers between devices: 56.5 us -> none  [passed_along(): return lax.ppermute(block, axis, route)]
    all_gather x2 -> x0, waiting for transfers between devices: 38.9 us -> none  [the longest x1 26.9 us: body(): lax.all_gather(mixed, 'tp', axis=1, tiled=True)]
    dot_general x10 -> x0, matrix products: 24.4 us -> none  [the longest x3 8.08 us: windowed(): jnp.einsum('nrhqk,nkrhd->nqrhd', weights, value_blocks, preferred_element...]
    slice x11 -> x0, local copies, waits for them, and re-layouts: 16.5 us -> none  [the longest x8 13.5 us: arrange(): return jnp.concatenate([whole[:-1], whole[1:]], axis=1)]
    unnamed x56 -> x5, local copies, waits for them, and re-layouts: 11.8 us -> 2.55 us
    ppermute x3 -> x0, starting transfers between devices: 7.62 us -> none  [passed_along(): return lax.ppermute(block, axis, route)]
    concatenate x2 -> x1, other arithmetic: 6.37 us -> 0.2 us  [body(): cos_table = jnp.concatenate([cosine, cosine], axis=1)]
  transfers between devices with their start and end apart: 5 -> 0, of which waited for: 4 -> 0; matrix products, arithmetic and copies ran while one was open for 18% -> 0% of each run, Pallas kernels for 0% -> 0%
where the time goes in v1:
time: 73.1 us; the launch traced here: 72.9 us
  Pallas kernels  69.1 us (95%)
  local copies, waits for them, and re-layouts  2.55 us (3%)
  other arithmetic  1.22 us (2%)
    pallas_call x1, Pallas kernels, body(): pl.pallas_call(functools.partial(kernel, n_sp, heads), out_shape=jax.Shap...  69.1 us
    unnamed x5, local copies, waits for them, and re-layouts  2.55 us

profile of v1, /device:TPU:19, one launch (start us, length us, event | category | flops | bytes accessed | tf_op | source)
XLA Modules:
  0.0 72.9 jit_solution(10350226841858852340)
XLA Ops:
  0.0 0.0 copy-start
  0.0 1.0 %fusion = (f32[512,64]{1,0:T(8,128)S(1)}, f32[512,64]{1,0:T(8,128)S(1)}, f32[512,64]{1,0:T(8,128)S(1)}) fusion(f32[64]{0:T(128)S(1)} %multiply_power_fusion, f32[512]{0:T(512)S(1)} %add_convert_fusion), kind=kLoop, calls=%fused_computation.4 | loop fusion | flops 65536 | bytes 395520 | tf_op jit(solution)/shard_map/neg | solution.py:303
  1.0 0.2 pad_maximum_fusion
  1.2 0.4 copy-done
  1.6 0.0 copy-start.1
  1.6 1.2 %copy-done.1 = bf16[256,2048]{1,0:T(8,128)(2,1)S(1)} copy-done((bf16[256,2048]{1,0:T(8,128)(2,1)S(1)}, bf16[256,2048]{1,0:T(8,128)(2,1)}, u32[]{:S(2)}) %copy-start.1) | copy-done | bytes 1048600
  2.8 69.1 %shard_map.55 = bf16[512,1024]{1,0:T(8,128)(2,1)S(1)} custom-call(bf16[256,2048]{1,0:T(8,128)(2,1)S(1)} %copy-done.1, bf16[2048,512]{1,0:T(8,128)(2,1)S(1)} %copy-done, bf16[2048,512]{1,0:T(8,128)(2,1)} %wk_hbm.1, bf16[2048,512]{1,0:T(8,128)(2,1)} %wv_hbm.1, bf16[1024,1024]{1,0:T(8,128)(2,1)} %wo_hbm.1, f32[512,128]{1,0:T(8,128)S(1)} %get-tuple-element.8.cos_ref, ...), custom_call_target="tpu_custom_call" | custom-call | tf_op jit(solution)/shard_map/pallas_call | solution.py:308
  71.9 1.0 %copy.7 = bf16[512,1024]{1,0:T(8,128)(2,1)} copy(bf16[512,1024]{1,0:T(8,128)(2,1)S(1)} %shard_map.55) | data formatting | bytes 2097152
  (2 shorter events, 0.0 us)
Async XLA Ops:
  0.0 1.6 %copy-start = (bf16[2048,512]{1,0:T(8,128)(2,1)S(1)}, bf16[2048,512]{1,0:T(8,128)(2,1)}, u32[]{:S(2)}) copy-start(bf16[2048,512]{1,0:T(8,128)(2,1)} %wq_hbm.1) | copy-start | bytes 6291460
  1.6 1.2 %copy-start.1 = (bf16[256,2048]{1,0:T(8,128)(2,1)S(1)}, bf16[256,2048]{1,0:T(8,128)(2,1)}, u32[]{:S(2)}) copy-start(bf16[256,2048]{1,0:T(8,128)(2,1)} %tok_hbm.1) | copy-start | bytes 3145732

commit v2 on v1

--- a/solution.py
+++ b/solution.py
@@ -2,6 +2,7 @@
 
 import jax
 import jax.numpy as jnp
+import numpy as np
 from jax import lax
 from jax.experimental import pallas as pl
 from jax.experimental.pallas import tpu as pltpu
@@ -17,8 +18,8 @@
 F32 = jnp.float32
 BF16 = jnp.bfloat16
 
-B, D, A, C, O = 0, 1, 2, 3, 4
-SLOTS = 5
+A, C, O = 0, 1, 2
+SLOTS = 3
 CLASSES = MIDDLE_DILATION
 CLASS_ROWS = 128
 
@@ -50,10 +51,11 @@
 
 def kernel(
     n_sp, heads,
-    tok_hbm, wq_hbm, wk_hbm, wv_hbm, wo_hbm, cos_ref, sin_ref,
+    tok_hbm, wq_hbm, wk_hbm, wv_hbm, wo_hbm, inv_hbm,
     out_ref,
-    tok, wkv, wq, wo, xg, ctx, q, k1, v1, perm, unperm, b16, b4, b1, mixp, mixg,
-    load_sem, x_sem, ctx_send, ctx_recv, mix_send, mix_recv,
+    tok, wkv, wq, wo, inv, cos_ref, sin_ref, xg, ctx, q, visitor, k1, v1, perm, unperm,
+    b16, b4, b1, near_out, near_lse, part, part_lse, far_out, far_lse, mixp, mixg,
+    load_sem, x_sem, ctx_send, ctx_recv, q_sem, part_sem, lse_sem, mix_send, mix_recv,
 ):
     sp = lax.axis_index("sp")
     tp = lax.axis_index("tp")
@@ -65,6 +67,8 @@
 
     tok_copy = pltpu.make_async_copy(tok_hbm, tok, load_sem.at[0])
     tok_copy.start()
+    inv_copy = pltpu.make_async_copy(inv_hbm, inv, load_sem.at[2 + 2 * heads + heads // 2])
+    inv_copy.start()
     kv_copies = []
     for h in range(heads):
         cols = pl.ds(h * HEAD, HEAD)
@@ -121,10 +125,24 @@
         device_id={"tp": other}, device_id_type=MESH)
     x_copy.start()
 
+    inv_copy.wait()
+    lane = iota((128, HEAD), 1)
+
+    def table(c, _):
+        positions = sp * 512 + spot(iota((128, HEAD), 0)) + c
+        angles = positions.astype(F32) * inv[...]
+        rows = pl.ds(pl.multiple_of(c * 128, 128), 128)
+        cos_ref[rows, :] = jnp.cos(angles)
+        sine = jnp.sin(angles)
+        sin_ref[rows, :] = jnp.where(lane < HEAD // 2, -sine, sine)
+        return 0
+
+    lax.fori_loop(0, CLASSES, table, 0)
+
     qi, kj = iota((128, 640), 0), iota((128, 640), 1)
     dist = 4 - (kj >> 7)
     diff = spot(qi) - spot(kj & 127) + 512 * dist
-    here = dist <= sp
+    here = (dist <= sp) | ((dist >= 3) & (dist <= sp + 2))
     far = here & ((diff & 15) == 0) & (diff >= 0) & (diff <= FAR_DILATION * REACH_STEPS)
     b16[...] = jnp.where(far, 0.0, NEG)
     mid = here & (diff >= 0) & (diff <= MIDDLE_DILATION * REACH_STEPS)
@@ -137,40 +155,55 @@
     col = iota((512, 512), 1)
     unperm[...] = jnp.where(spot(col & 127) + (col >> 7) == iota((512, 512), 0), 1.0, 0.0).astype(BF16)
 
-    for slot in (B, D, A, C):
-        @pl.when(sp < 4 - slot)
+    for slot in (A, C):
+        @pl.when(sp < 2 - slot)
         def _():
             def clear(h, _):
                 ctx[h, :, :, slot] = jnp.zeros((2, CLASSES, 128, HEAD), BF16)
                 return 0
             lax.fori_loop(0, heads, clear, 0)
 
+    part_lse[...] = jnp.zeros(part_lse.shape, F32)
+
+    @pl.when(z == 0)
+    def _():
+        far_out[...] = jnp.zeros(far_out.shape, BF16)
+        far_lse[...] = jnp.full(far_lse.shape, NEG, F32)
+
+    def remote(src, dst, send_sem, recv_sem, ids):
+        return pltpu.make_async_remote_copy(
+            src_ref=src, dst_ref=dst, send_sem=send_sem, recv_sem=recv_sem,
+            device_id=ids, device_id_type=MESH)
+
+    down = {"sp": sp + 2}
+    up = {"sp": sp - 2}
+    side = {"sp": y_partner}
+
     def send(h, src, dst, ids):
-        return pltpu.make_async_remote_copy(
-            src_ref=ctx.at[h, :, :, src], dst_ref=ctx.at[h, :, :, dst],
-            send_sem=ctx_send.at[dst, h], recv_sem=ctx_recv.at[dst, h],
-            device_id=ids, device_id_type=MESH)
-
-    down = {"sp": sp + 2}
-    side = {"sp": y_partner}
-
-    def sends_of(h, src):
-        if src == O:
-            return [(has_next, send(h, O, A, down)), (even, send(h, O, C, side))]
-        if src == A:
-            return [(has_next & (z > 0), send(h, A, B, down)),
-                    (even & (z > 0), send(h, A, D, side)),
-                    ((odd == 1) & (z > 0), send(h, A, C, side))]
-        return [((odd == 1) & (z > 1), send(h, B, D, side))]
-
-    def start_all(h, src):
-        for condition, copy in sends_of(h, src):
+        return remote(ctx.at[h, :, :, src], ctx.at[h, :, :, dst],
+                      ctx_send.at[dst, h], ctx_recv.at[dst, h], ids)
+
+    def send_own(h):
+        return ((has_next, send(h, O, A, down)), (even, send(h, O, C, side)))
+
+    def send_relay(h):
+        return (((odd == 1) & (z > 0), send(h, A, C, side)),)
+
+    def send_query(h):
+        return ((z > 0, remote(q.at[h], visitor.at[h], q_sem.at[0, h], q_sem.at[1, h], up)),)
+
+    def send_part(h):
+        return ((has_next, remote(part.at[h], far_out.at[h], part_sem.at[0, h], part_sem.at[1, h], down)),
+                (has_next, remote(part_lse.at[h], far_lse.at[h], lse_sem.at[0, h], lse_sem.at[1, h], down)))
+
+    def start_all(sends):
+        for condition, copy in sends:
             @pl.when(condition)
             def _():
                 copy.start()
 
     def receive(h, slot):
-        @pl.when(sp >= 4 - slot)
+        @pl.when(sp >= 2 - slot)
         def _():
             send(h, slot, slot, side).wait_recv()
 
@@ -184,7 +217,7 @@
         k = rotated(kv[:, :HEAD], cos_ref[...], sin_ref[...]).astype(BF16)
         ctx[h, 0, :, O] = k.reshape(CLASSES, 128, HEAD)
         ctx[h, 1, :, O] = kv[:, HEAD:].astype(BF16).reshape(CLASSES, 128, HEAD)
-        start_all(h, O)
+        start_all(send_own(h))
         return 0
 
     for pair in kv_copies:
@@ -200,16 +233,10 @@
         for s in range(2):
             r = rotated(qq[:, s * HEAD:(s + 1) * HEAD], cos_ref[...], sin_ref[...])
             q[2 * p + s] = r.astype(BF16).reshape(CLASSES, 128, HEAD)
+            start_all(send_query(2 * p + s))
         return 0
 
     lax.fori_loop(0, heads // 2, project_q, 0)
-
-    def relay(h, _):
-        receive(h, A)
-        start_all(h, A)
-        return 0
-
-    lax.fori_loop(0, heads, relay, 0)
 
     def mix_copy(h):
         cols = pl.ds(pl.multiple_of(h * HEAD, HEAD), HEAD)
@@ -218,11 +245,27 @@
             send_sem=mix_send.at[h], recv_sem=mix_recv.at[h],
             device_id={"tp": other}, device_id_type=MESH)
 
-    def attend(h, _):
-        receive(h, B)
-        start_all(h, B)
-        receive(h, C)
-        receive(h, D)
+    eye = iota((128, 128), 0) == iota((128, 128), 1)
+
+    def visit(h):
+        @pl.when(has_next)
+        def _():
+            remote(q.at[h], visitor.at[h], q_sem.at[0, h], q_sem.at[1, h], side).wait_recv()
+
+            def of_class(c, _):
+                keys = ctx[h, 0, c, A:O].reshape(2 * 128, HEAD)
+                vals = ctx[h, 1, c, A:O].reshape(2 * 128, HEAD)
+                scores = transposed_dot(visitor[h, c], keys) * HEAD ** (-0.5)
+                result, lse = softmax(scores + b16[:, :256], vals)
+                part[h, c] = result.astype(BF16)
+                part_lse[h, pl.ds(c, 1), :] = jnp.sum(jnp.where(eye, lse, 0.0), axis=0, keepdims=True)
+                return 0
+
+            lax.fori_loop(0, CLASSES, of_class, 0)
+
+        start_all(send_part(h))
+
+    def attend(h):
         tail = unperm[384:512, :]
         for kv, near in ((0, k1), (1, v1)):
             last = ctx[h, kv, :, C].reshape(512, HEAD)
@@ -234,24 +277,55 @@
             keys = ctx[h, 0, c].reshape(SLOTS * 128, HEAD)
             vals = ctx[h, 1, c].reshape(SLOTS * 128, HEAD)
             scores = transposed_dot(qc, keys) * HEAD ** (-0.5)
-            r16, l16 = softmax(scores + b16[...], vals)
-            r4, l4 = softmax(scores[:, 384:] + b4[...], vals[384:])
+            r16, l16 = softmax(scores + b16[:, 256:], vals)
+            r4, l4 = softmax(scores[:, 128:] + b4[...], vals[128:])
             r1, l1 = softmax(transposed_dot(qc, k1[...]) * HEAD ** (-0.5) + b1[c], v1[...])
             most = jnp.maximum(jnp.maximum(l16, l4), l1)
             e16, e4, e1 = jnp.exp(l16 - most), jnp.exp(l4 - most), jnp.exp(l1 - most)
-            share = 1.0 / (e16 + e4 + e1)
-            mixed = r1 * (e1 * share) + r4 * (e4 * share) + r16 * (e16 * share)
-            mixp[pl.ds(pl.multiple_of(c * 128, 128), 128), :] = mixed.astype(BF16)
+            total = e16 + e4 + e1
+            share = 1.0 / total
+            near_out[h, c] = r1 * (e1 * share) + r4 * (e4 * share) + r16 * (e16 * share)
+            near_lse[h, c] = jnp.broadcast_to(most + jnp.log(total), (128, HEAD))
             return 0
 
         lax.fori_loop(0, CLASSES, of_class, 0)
+
+    def step(h, _):
+        @pl.when(h < heads)
+        def _():
+            receive(h, A)
+            start_all(send_relay(h))
+
+        @pl.when(h > 0)
+        def _():
+            receive(h - 1, C)
+            visit(h - 1)
+            attend(h - 1)
+        return 0
+
+    lax.fori_loop(0, heads + 1, step, 0)
+
+    def combine(h, _):
+        @pl.when(z > 0)
+        def _():
+            remote(part.at[h], far_out.at[h], part_sem.at[0, h], part_sem.at[1, h], side).wait_recv()
+            remote(part_lse.at[h], far_lse.at[h], lse_sem.at[0, h], lse_sem.at[1, h], side).wait_recv()
+
+        for c in range(CLASSES):
+            row = far_lse[h, c:c + 1, :]
+            lf = jnp.sum(jnp.where(eye, row, 0.0), axis=1, keepdims=True)
+            ln = near_lse[h, c]
+            most = jnp.maximum(ln, lf)
+            en, ef = jnp.exp(ln - most), jnp.exp(lf - most)
+            mixed = (near_out[h, c] * en + far_out[h, c].astype(F32) * ef) / (en + ef)
+            mixp[c * 128:(c + 1) * 128, :] = mixed.astype(BF16)
         natural = jnp.dot(unperm[...], mixp[...], preferred_element_type=F32).astype(BF16)
         cols = pl.ds(pl.multiple_of(h * HEAD, HEAD), HEAD)
         mixg[tp, :, cols] = natural
         mix_copy(h).start()
         return 0
 
-    lax.fori_loop(0, heads, attend, 0)
+    lax.fori_loop(0, heads, combine, 0)
 
     wo_copy.wait()
 
@@ -274,8 +348,8 @@
     x_copy.wait_send()
 
     def left(h, _):
-        for src in (O, A, B):
-            for condition, copy in sends_of(h, src):
+        for sends in (send_own(h), send_relay(h), send_query(h), send_part(h)):
+            for condition, copy in sends:
                 @pl.when(condition)
                 def _():
                     copy.wait_send()
@@ -293,14 +367,9 @@
     assert rows * 4 == FAR_DILATION * REACH_STEPS and rows == 512
     assert n_sp % 2 == 0 and lax.axis_size("tp") == 2 and heads % 2 == 0
 
-    index = jnp.arange(rows, dtype=jnp.int32)
-    positions = lax.axis_index("sp") * rows + spot(index & 127) + (index >> 7)
     half = HEAD // 2
-    inverse = THETA_BASE ** (-jnp.arange(half, dtype=F32) / half)
-    angles = positions.astype(F32)[:, None] * inverse
-    cosine, sine = jnp.cos(angles), jnp.sin(angles)
-    cos_table = jnp.concatenate([cosine, cosine], axis=1)
-    sin_table = jnp.concatenate([-sine, sine], axis=1)
+    inverse = THETA_BASE ** (-np.arange(half, dtype=np.float64) / half)
+    inverse = np.concatenate([inverse, inverse]).astype(np.float32)[None, :]
 
     anywhere = pl.BlockSpec(memory_space=pl.ANY)
     vmem = pl.BlockSpec(memory_space=pltpu.VMEM)
@@ -308,15 +377,19 @@
     return pl.pallas_call(
         functools.partial(kernel, n_sp, heads),
         out_shape=jax.ShapeDtypeStruct((rows, out_cols), BF16),
-        in_specs=[anywhere] * 5 + [vmem] * 2,
+        in_specs=[anywhere] * 6,
         out_specs=vmem,
         scratch_shapes=[
             pltpu.VMEM((half_rows, width), BF16),
             pltpu.VMEM((heads, width, 2 * HEAD), BF16),
             pltpu.VMEM((heads // 2, width, 2 * HEAD), BF16),
             pltpu.VMEM(output_weight.shape, BF16),
+            pltpu.VMEM((1, HEAD), F32),
+            pltpu.VMEM((rows, HEAD), F32),
+            pltpu.VMEM((rows, HEAD), F32),
             pltpu.VMEM((CLASSES, 2, 64, width), BF16),
             pltpu.VMEM((heads, 2, CLASSES, SLOTS, 128, HEAD), BF16),
+            pltpu.VMEM((heads, CLASSES, 128, HEAD), BF16),
             pltpu.VMEM((heads, CLASSES, 128, HEAD), BF16),
             pltpu.VMEM((640, HEAD), BF16),
             pltpu.VMEM((640, HEAD), BF16),
@@ -325,19 +398,28 @@
             pltpu.VMEM((128, 640), F32),
             pltpu.VMEM((128, 256), F32),
             pltpu.VMEM((CLASSES, 128, 640), F32),
+            pltpu.VMEM((heads, CLASSES, 128, HEAD), F32),
+            pltpu.VMEM((heads, CLASSES, 128, HEAD), F32),
+            pltpu.VMEM((heads, CLASSES, 128, HEAD), BF16),
+            pltpu.VMEM((heads, 8, 128), F32),
+            pltpu.VMEM((heads, CLASSES, 128, HEAD), BF16),
+            pltpu.VMEM((heads, 8, 128), F32),
             pltpu.VMEM((512, HEAD), BF16),
             pltpu.VMEM((2, rows, heads * HEAD), BF16),
-            pltpu.SemaphoreType.DMA((2 + 2 * heads + heads // 2,)),
+            pltpu.SemaphoreType.DMA((3 + 2 * heads + heads // 2,)),
             pltpu.SemaphoreType.DMA((2,)),
-            pltpu.SemaphoreType.DMA((4, heads)),
-            pltpu.SemaphoreType.DMA((4, heads)),
+            pltpu.SemaphoreType.DMA((2, heads)),
+            pltpu.SemaphoreType.DMA((2, heads)),
+            pltpu.SemaphoreType.DMA((2, heads)),
+            pltpu.SemaphoreType.DMA((2, heads)),
+            pltpu.SemaphoreType.DMA((2, heads)),
             pltpu.SemaphoreType.DMA((heads,)),
             pltpu.SemaphoreType.DMA((heads,)),
         ],
         compiler_params=pltpu.CompilerParams(
             collective_id=0, has_side_effects=True, vmem_limit_bytes=48 * 1024 * 1024
         ),
-    )(tokens, query_weight, key_weight, value_weight, output_weight, cos_table, sin_table)
+    )(tokens, query_weight, key_weight, value_weight, output_weight, jnp.asarray(inverse))
 
 
 def solution(mesh):

time: 73.1 us -> 55.9 us (0.76)
  Pallas kernels: 69.1 us -> 51.2 us
  local copies, waits for them, and re-layouts: 2.55 us -> 4.44 us
  other arithmetic: 1.22 us -> 0 us
    pallas_call x1, Pallas kernels: 69.1 us -> 51.2 us  [body(): pl.pallas_call(functools.partial(kernel, n_sp, heads), out_shape=jax.Shap...]
    unnamed x5 -> x7, local copies, waits for them, and re-layouts: 2.55 us -> 4.44 us
    neg x1 -> x0, other arithmetic: 0.99 us -> none  [body(): sin_table = jnp.concatenate([-sine, sine], axis=1)]
where the time goes in v2:
time: 55.9 us; the launch traced here: 55.7 us
  Pallas kernels  51.2 us (92%)
  local copies, waits for them, and re-layouts  4.44 us (8%)
    pallas_call x1, Pallas kernels, body(): pl.pallas_call(functools.partial(kernel, n_sp, heads), out_shape=jax.Shap...  51.2 us
    unnamed x7, local copies, waits for them, and re-layouts  4.44 us

profile of v2, /device:TPU:19, one launch (start us, length us, event | category | flops | bytes accessed | tf_op | source)
XLA Modules:
  0.0 55.7 jit_solution(8073157795008690068)
XLA Ops:
  0.0 0.0 copy-start
  0.0 1.6 %copy-done = bf16[2048,512]{1,0:T(8,128)(2,1)S(1)} copy-done((bf16[2048,512]{1,0:T(8,128)(2,1)S(1)}, bf16[2048,512]{1,0:T(8,128)(2,1)}, u32[]{:S(2)}) %copy-start) | copy-done | bytes 2097176
  1.6 0.0 copy-start.1
  1.6 1.2 %copy-done.1 = bf16[256,2048]{1,0:T(8,128)(2,1)S(1)} copy-done((bf16[256,2048]{1,0:T(8,128)(2,1)S(1)}, bf16[256,2048]{1,0:T(8,128)(2,1)}, u32[]{:S(2)}) %copy-start.1) | copy-done | bytes 1048600
  2.8 0.0 copy-start.2
  2.8 0.7 %copy-done.2 = f32[1,128]{1,0:T(1,128)S(1)} copy-done((f32[1,128]{1,0:T(1,128)S(1)}, f32[1,128]{1,0:T(1,128)}, u32[]{:S(2)}) %copy-start.2) | copy-done | bytes 536
  3.5 51.2 %shard_map.64 = bf16[512,1024]{1,0:T(8,128)(2,1)S(1)} custom-call(bf16[256,2048]{1,0:T(8,128)(2,1)S(1)} %copy-done.1, bf16[2048,512]{1,0:T(8,128)(2,1)S(1)} %copy-done, bf16[2048,512]{1,0:T(8,128)(2,1)} %wk_hbm.1, bf16[2048,512]{1,0:T(8,128)(2,1)} %wv_hbm.1, bf16[1024,1024]{1,0:T(8,128)(2,1)} %wo_hbm.1, f32[1,128]{1,0:T(1,128)S(1)} %copy-done.2), custom_call_target="tpu_custom_call" | custom-call | tf_op jit(solution)/shard_map/pallas_call | solution.py:377
  54.7 1.0 %copy.8 = bf16[512,1024]{1,0:T(8,128)(2,1)} copy(bf16[512,1024]{1,0:T(8,128)(2,1)S(1)} %shard_map.64) | data formatting | bytes 2097152
Async XLA Ops:
  0.0 1.6 %copy-start = (bf16[2048,512]{1,0:T(8,128)(2,1)S(1)}, bf16[2048,512]{1,0:T(8,128)(2,1)}, u32[]{:S(2)}) copy-start(bf16[2048,512]{1,0:T(8,128)(2,1)} %wq_hbm.1) | copy-start | bytes 6291460
  1.6 1.2 %copy-start.1 = (bf16[256,2048]{1,0:T(8,128)(2,1)S(1)}, bf16[256,2048]{1,0:T(8,128)(2,1)}, u32[]{:S(2)}) copy-start(bf16[256,2048]{1,0:T(8,128)(2,1)} %tok_hbm.1) | copy-start | bytes 3145732
  2.8 0.7 %copy-start.2 = (f32[1,128]{1,0:T(1,128)S(1)}, f32[1,128]{1,0:T(1,128)}, u32[]{:S(2)}) copy-start(f32[1,128]{1,0:T(1,128)} %constant.2.clone.inv_hbm) | copy-start | bytes 1540

commit v3 on v2

--- a/solution.py
+++ b/solution.py
@@ -54,7 +54,7 @@
     tok_hbm, wq_hbm, wk_hbm, wv_hbm, wo_hbm, inv_hbm,
     out_ref,
     tok, wkv, wq, wo, inv, cos_ref, sin_ref, xg, ctx, q, visitor, k1, v1, perm, unperm,
-    b16, b4, b1, near_out, near_lse, part, part_lse, far_out, far_lse, mixp, mixg,
+    b16, b4, b1, near_out, near_lse, part, part_lse, far_out, far_lse, mixp, mixg, out_sum,
     load_sem, x_sem, ctx_send, ctx_recv, q_sem, part_sem, lse_sem, mix_send, mix_recv,
 ):
     sp = lax.axis_index("sp")
@@ -139,6 +139,74 @@
 
     lax.fori_loop(0, CLASSES, table, 0)
 
+    def remote(src, dst, send_sem, recv_sem, ids):
+        return pltpu.make_async_remote_copy(
+            src_ref=src, dst_ref=dst, send_sem=send_sem, recv_sem=recv_sem,
+            device_id=ids, device_id_type=MESH)
+
+    down = {"sp": sp + 2}
+    up = {"sp": sp - 2}
+    side = {"sp": y_partner}
+
+    def send(h, src, dst, ids):
+        return remote(ctx.at[h, :, :, src], ctx.at[h, :, :, dst],
+                      ctx_send.at[dst, h], ctx_recv.at[dst, h], ids)
+
+    def send_own(h):
+        return ((has_next, send(h, O, A, down)), (even, send(h, O, C, side)))
+
+    def send_relay(h):
+        return (((odd == 1) & (z > 0), send(h, A, C, side)),)
+
+    def send_query(h):
+        return ((z > 0, remote(q.at[h], visitor.at[h], q_sem.at[0, h], q_sem.at[1, h], up)),)
+
+    def send_part(h):
+        return ((has_next, remote(part.at[h], far_out.at[h], part_sem.at[0, h], part_sem.at[1, h], down)),
+                (has_next, remote(part_lse.at[h], far_lse.at[h], lse_sem.at[0, h], lse_sem.at[1, h], down)))
+
+    def start_all(sends):
+        for condition, copy in sends:
+            @pl.when(condition)
+            def _():
+                copy.start()
+
+    def receive(h, slot):
+        @pl.when(sp >= 2 - slot)
+        def _():
+            send(h, slot, slot, side).wait_recv()
+
+    x_copy.wait_recv()
+
+    def tokens():
+        return xg[...].reshape(512, width)
+
+    def project_kv(h, _):
+        kv = jnp.dot(tokens(), wkv[h], preferred_element_type=F32)
+        k = rotated(kv[:, :HEAD], cos_ref[...], sin_ref[...]).astype(BF16)
+        ctx[h, 0, :, O] = k.reshape(CLASSES, 128, HEAD)
+        ctx[h, 1, :, O] = kv[:, HEAD:].astype(BF16).reshape(CLASSES, 128, HEAD)
+        start_all(send_own(h))
+        return 0
+
+    for pair in kv_copies:
+        for copy in pair:
+            copy.wait()
+    lax.fori_loop(0, heads, project_kv, 0)
+
+    for copy in q_copies:
+        copy.wait()
+
+    def project_q(p, _):
+        qq = jnp.dot(tokens(), wq[p], preferred_element_type=F32)
+        for s in range(2):
+            r = rotated(qq[:, s * HEAD:(s + 1) * HEAD], cos_ref[...], sin_ref[...])
+            q[2 * p + s] = r.astype(BF16).reshape(CLASSES, 128, HEAD)
+            start_all(send_query(2 * p + s))
+        return 0
+
+    lax.fori_loop(0, heads // 2, project_q, 0)
+
     qi, kj = iota((128, 640), 0), iota((128, 640), 1)
     dist = 4 - (kj >> 7)
     diff = spot(qi) - spot(kj & 127) + 512 * dist
@@ -170,74 +238,6 @@
         far_out[...] = jnp.zeros(far_out.shape, BF16)
         far_lse[...] = jnp.full(far_lse.shape, NEG, F32)
 
-    def remote(src, dst, send_sem, recv_sem, ids):
-        return pltpu.make_async_remote_copy(
-            src_ref=src, dst_ref=dst, send_sem=send_sem, recv_sem=recv_sem,
-            device_id=ids, device_id_type=MESH)
-
-    down = {"sp": sp + 2}
-    up = {"sp": sp - 2}
-    side = {"sp": y_partner}
-
-    def send(h, src, dst, ids):
-        return remote(ctx.at[h, :, :, src], ctx.at[h, :, :, dst],
-                      ctx_send.at[dst, h], ctx_recv.at[dst, h], ids)
-
-    def send_own(h):
-        return ((has_next, send(h, O, A, down)), (even, send(h, O, C, side)))
-
-    def send_relay(h):
-        return (((odd == 1) & (z > 0), send(h, A, C, side)),)
-
-    def send_query(h):
-        return ((z > 0, remote(q.at[h], visitor.at[h], q_sem.at[0, h], q_sem.at[1, h], up)),)
-
-    def send_part(h):
-        return ((has_next, remote(part.at[h], far_out.at[h], part_sem.at[0, h], part_sem.at[1, h], down)),
-                (has_next, remote(part_lse.at[h], far_lse.at[h], lse_sem.at[0, h], lse_sem.at[1, h], down)))
-
-    def start_all(sends):
-        for condition, copy in sends:
-            @pl.when(condition)
-            def _():
-                copy.start()
-
-    def receive(h, slot):
-        @pl.when(sp >= 2 - slot)
-        def _():
-            send(h, slot, slot, side).wait_recv()
-
-    x_copy.wait_recv()
-
-    def tokens():
-        return xg[...].reshape(512, width)
-
-    def project_kv(h, _):
-        kv = jnp.dot(tokens(), wkv[h], preferred_element_type=F32)
-        k = rotated(kv[:, :HEAD], cos_ref[...], sin_ref[...]).astype(BF16)
-        ctx[h, 0, :, O] = k.reshape(CLASSES, 128, HEAD)
-        ctx[h, 1, :, O] = kv[:, HEAD:].astype(BF16).reshape(CLASSES, 128, HEAD)
-        start_all(send_own(h))
-        return 0
-
-    for pair in kv_copies:
-        for copy in pair:
-            copy.wait()
-    lax.fori_loop(0, heads, project_kv, 0)
-
-    for copy in q_copies:
-        copy.wait()
-
-    def project_q(p, _):
-        qq = jnp.dot(tokens(), wq[p], preferred_element_type=F32)
-        for s in range(2):
-            r = rotated(qq[:, s * HEAD:(s + 1) * HEAD], cos_ref[...], sin_ref[...])
-            q[2 * p + s] = r.astype(BF16).reshape(CLASSES, 128, HEAD)
-            start_all(send_query(2 * p + s))
-        return 0
-
-    lax.fori_loop(0, heads // 2, project_q, 0)
-
     def mix_copy(h):
         cols = pl.ds(pl.multiple_of(h * HEAD, HEAD), HEAD)
         return pltpu.make_async_remote_copy(
@@ -300,12 +300,15 @@
         def _():
             receive(h - 1, C)
             visit(h - 1)
+
+        @pl.when((h > 0) & (h < heads))
+        def _():
             attend(h - 1)
         return 0
 
     lax.fori_loop(0, heads + 1, step, 0)
 
-    def combine(h, _):
+    def combine(h):
         @pl.when(z > 0)
         def _():
             remote(part.at[h], far_out.at[h], part_sem.at[0, h], part_sem.at[1, h], side).wait_recv()
@@ -323,24 +326,44 @@
         cols = pl.ds(pl.multiple_of(h * HEAD, HEAD), HEAD)
         mixg[tp, :, cols] = natural
         mix_copy(h).start()
-        return 0
-
-    lax.fori_loop(0, heads, combine, 0)
-
-    wo_copy.wait()
 
     def gathered(h, _):
         mix_copy(h).wait_recv()
         return 0
 
-    lax.fori_loop(0, heads, gathered, 0)
     half = mixg.shape[2]
+    first = half // 2
+
+    def partial_out(i, _):
+        cols = pl.ds(pl.multiple_of(i * 256, 256), 256)
+        total = jnp.dot(mixg[0, :, :first], wo[:first, cols], preferred_element_type=F32)
+        total = total + jnp.dot(mixg[1, :, :first], wo[half:half + first, cols], preferred_element_type=F32)
+        out_sum[:, cols] = total
+        return 0
+
+    def finish(h, _):
+        @pl.when(h == heads - 2)
+        def _():
+            attend(heads - 1)
+
+        @pl.when(h == heads - 1)
+        def _():
+            wo_copy.wait()
+            lax.fori_loop(0, heads // 2, gathered, 0)
+            lax.fori_loop(0, out_ref.shape[1] // 256, partial_out, 0)
+
+        combine(h)
+        return 0
+
+    lax.fori_loop(0, heads, finish, 0)
+
+    lax.fori_loop(heads // 2, heads, gathered, 0)
 
     def project_out(i, _):
         cols = pl.ds(pl.multiple_of(i * 256, 256), 256)
-        total = jnp.dot(mixg[0], wo[:half, cols], preferred_element_type=F32)
-        total = total + jnp.dot(mixg[1], wo[half:, cols], preferred_element_type=F32)
-        out_ref[:, cols] = total.astype(BF16)
+        total = jnp.dot(mixg[0, :, first:], wo[first:half, cols], preferred_element_type=F32)
+        total = total + jnp.dot(mixg[1, :, first:], wo[half + first:, cols], preferred_element_type=F32)
+        out_ref[:, cols] = (out_sum[:, cols] + total).astype(BF16)
         return 0
 
     lax.fori_loop(0, out_ref.shape[1] // 256, project_out, 0)
@@ -365,7 +388,7 @@
     rows = half_rows * lax.axis_size("tp")
     heads = query_weight.shape[1] // HEAD
     assert rows * 4 == FAR_DILATION * REACH_STEPS and rows == 512
-    assert n_sp % 2 == 0 and lax.axis_size("tp") == 2 and heads % 2 == 0
+    assert n_sp % 2 == 0 and lax.axis_size("tp") == 2 and heads % 2 == 0 and heads >= 4
 
     half = HEAD // 2
     inverse = THETA_BASE ** (-np.arange(half, dtype=np.float64) / half)
@@ -406,6 +429,7 @@
             pltpu.VMEM((heads, 8, 128), F32),
             pltpu.VMEM((512, HEAD), BF16),
             pltpu.VMEM((2, rows, heads * HEAD), BF16),
+            pltpu.VMEM((rows, out_cols), F32),
             pltpu.SemaphoreType.DMA((3 + 2 * heads + heads // 2,)),
             pltpu.SemaphoreType.DMA((2,)),
             pltpu.SemaphoreType.DMA((2, heads)),
@@ -417,7 +441,7 @@
             pltpu.SemaphoreType.DMA((heads,)),
         ],
         compiler_params=pltpu.CompilerParams(
-            collective_id=0, has_side_effects=True, vmem_limit_bytes=48 * 1024 * 1024
+            collective_id=0, has_side_effects=True, vmem_limit_bytes=63 * 1024 * 1024
         ),
     )(tokens, query_weight, key_weight, value_weight, output_weight, jnp.asarray(inverse))
 

time: 55.9 us -> 55.1 us (0.986)
  local copies, waits for them, and re-layouts: 4.44 us -> 2.26 us
  Pallas kernels: 51.2 us -> 52.7 us
    unnamed x7 -> x1, local copies, waits for them, and re-layouts: 4.44 us -> 2.26 us
    pallas_call x1, Pallas kernels: 51.2 us -> 52.7 us  [body(): pl.pallas_call(functools.partial(kernel, n_sp, heads), out_shape=jax.Shap...]
where the time goes in v3:
time: 55.1 us; the launch traced here: 55 us
  Pallas kernels  52.7 us (96%)
  local copies, waits for them, and re-layouts  2.26 us (4%)
    pallas_call x1, Pallas kernels, body(): pl.pallas_call(functools.partial(kernel, n_sp, heads), out_shape=jax.Shap...  52.7 us
    unnamed x1, local copies, waits for them, and re-layouts  2.26 us

profile of v3, /device:TPU:19, one launch (start us, length us, event | category | flops | bytes accessed | tf_op | source)
XLA Modules:
  0.0 55.0 jit_solution(14728148728564380338)
XLA Ops:
  0.0 52.7 %shard_map.64 = bf16[512,1024]{1,0:T(8,128)(2,1)} custom-call(bf16[256,2048]{1,0:T(8,128)(2,1)} %tok_hbm.1, bf16[2048,512]{1,0:T(8,128)(2,1)} %wq_hbm.1, bf16[2048,512]{1,0:T(8,128)(2,1)} %wk_hbm.1, bf16[2048,512]{1,0:T(8,128)(2,1)} %wv_hbm.1, bf16[1024,1024]{1,0:T(8,128)(2,1)} %wo_hbm.1, f32[1,128]{1,0:T(1,128)} %constant.2.clone.inv_hbm), custom_call_target="tpu_custom_call" | custom-call | tf_op jit(solution)/shard_map/pallas_call | solution.py:400
  52.7 2.3 %copy.8 = bf16[512,1024]{1,0:T(8,128)(2,1)} copy(bf16[512,1024]{1,0:T(8,128)(2,1)} %shard_map.64) | data formatting | bytes 2097152
